TPU v7x, 32 devices: a whole 2x2x4 slice. The times are simulated.
32 devices in a mesh: rep: 4 (over z), fs: 4 (over y, x), tp: 2 (over core).
Axes of the slice: x: 2, y: 2, z: 4, core: 2. Of those that a mesh axis runs over, the one named last changes fastest.
Arguments:
- tokens: bfloat16 [16, 768, 2048], P(('rep', 'fs')), may hold values from -6 to 6
- norm_gain: float32 [2048], replicated, may hold values from 0.1 to 1.9
- outer_weight: bfloat16 [2048, 2048], P('fs', 'tp'), may hold values from -0.125 to 0.125
- inner_weight: bfloat16 [2048, 2048], P('fs', 'tp'), may hold values from -0.125 to 0.125
- value_weight: bfloat16 [2048, 2048], P('fs', 'tp'), may hold values from -0.125 to 0.125
- conv_taps: float32 [3, 2048], replicated, may hold values from -3.5 to 3.5
- out_weight: bfloat16 [2048, 2048], P('fs', 'tp'), may hold values from -0.125 to 0.125
Outputs:
- mixed: bfloat16 [16, 768, 2048], P(('rep', 'fs'), None, 'tp')
All inputs are finite; a program needn't handle non-finite values.
Results may differ from a plain program's by a relative error of at most 0.014.
Values may be sent and summed in bfloat16 or wider, within the bound.
A program may use at most 64 MiB of HBM per device.

v0:
```python
import jax
import jax.numpy as jnp
from jax import lax
from jax.sharding import PartitionSpec as P


def local(tokens, norm_gain, outer_weight, inner_weight, value_weight, conv_taps, out_weight):
    seq_len = tokens.shape[1]
    width = tokens.shape[2]
    xf = tokens.reshape(seq_len, width).astype(jnp.float32)
    scale = lax.rsqrt(jnp.mean(xf * xf, axis=-1, keepdims=True) + 1e-06)
    normed = (xf * scale * norm_gain).astype(jnp.bfloat16)
    columns = outer_weight.shape[1]

    def add_piece(piece):
        return jnp.dot(normed, piece, preferred_element_type=jnp.float32)

    outer = add_piece(lax.all_gather(outer_weight, "fs", axis=0, tiled=True))
    inner = add_piece(lax.all_gather(inner_weight, "fs", axis=0, tiled=True))
    value = add_piece(lax.all_gather(value_weight, "fs", axis=0, tiled=True))
    outer = outer.astype(jnp.bfloat16)
    inner = inner.astype(jnp.bfloat16)
    value = value.astype(jnp.bfloat16)
    product = inner.astype(jnp.float32) * value.astype(jnp.float32)
    offset = lax.axis_index("tp") * columns
    taps = lax.dynamic_slice_in_dim(conv_taps, offset, columns, 1)
    count = conv_taps.shape[0]
    padded = jnp.pad(product, ((count - 1, 0), (0, 0)))
    convolved = jnp.zeros((seq_len, columns), jnp.float32)
    for k in range(count):
        convolved = convolved + taps[k] * padded[k : k + seq_len, :]
    gated = (outer.astype(jnp.float32) * convolved).astype(jnp.bfloat16)
    everything = lax.all_gather(gated, "tp", axis=1, tiled=True)
    result = jnp.dot(
        everything,
        lax.all_gather(out_weight, "fs", axis=0, tiled=True),
        preferred_element_type=jnp.float32,
    )
    return result.astype(jnp.bfloat16).reshape(1, seq_len, columns)


def solution(mesh):
    in_specs = (
        P(("rep", "fs"), None, None),
        P(),
        P("fs", "tp"),
        P("fs", "tp"),
        P("fs", "tp"),
        P(),
        P("fs", "tp"),
    )
    out_specs = P(("rep", "fs"), None, "tp")
    return jax.shard_map(local, mesh=mesh, in_specs=in_specs, out_specs=out_specs, check_vma=False)
```

profile of v0, /device:TPU:0, one launch (start us, length us, event | category | flops | bytes accessed | tf_op | source)
XLA Modules:
  0.0 255.5 jit_solution(18304229545955920664)
XLA Ops:
  6.5 0.0 copy-start
  6.5 0.0 all-gather.8.cloned.1.call-start
  6.5 0.7 all-gather.8.cloned.1.call-update
  7.3 0.0 copy-start.1
  7.3 0.0 all-gather.10.cloned.1.call-start
  7.3 0.7 all-gather.10.cloned.1.call-update
  8.0 0.0 all-gather.6.cloned.1.call-start
  8.1 0.7 all-gather.6.cloned.1.call-update
  8.8 0.0 all-gather.14.cloned.1.call-start
  8.8 0.5 all-gather.14.cloned.1.call-update
  9.3 0.0 all-gather.12.cloned.1.call-start
  9.4 0.9 constant_dynamic-slice_fusion
  10.3 0.0 copy-done
  10.3 0.7 fusion
  11.0 53.5 %all-gather.8.cloned.1.call-done = bf16[2048,1024]{1,0:T(8,128)(2,1)} async-done(((bf16[512,1024]{1,0:T(8,128)(2,1)}), bf16[2048,1024]{1,0:T(8,128)(2,1)}) %all-gather.8.cloned.1.call-update) | async-done | bytes 4194320 | tf_op jit(solution)/shard_map/all_gather | solution.py:19
  64.5 0.0 copy-done.1
  64.5 6.8 %convolution_convert_fusion.2 = bf16[768,1024]{1,0:T(8,128)(2,1)} fusion(bf16[2048,1024]{1,0:T(8,128)(2,1)} %all-gather.8.cloned.1.call-done, bf16[1,768,2048]{2,1,0:T(8,128)(2,1)S(1)} %copy-done, f32[2048]{0:T(1024)S(1)} %copy-done.1, f32[768]{0:T(1024)S(1)} %add_rsqrt_fusion), kind=kOutput, calls=%fused_computation.9 | convolution fusion | flops 3228303360 | bytes 8924160 | tf_op jit(solution)/shard_map/dot_general | solution.py:16
  71.3 47.6 %all-gather.10.cloned.1.call-done = bf16[2048,1024]{1,0:T(8,128)(2,1)} async-done(((bf16[512,1024]{1,0:T(8,128)(2,1)}), bf16[2048,1024]{1,0:T(8,128)(2,1)}) %all-gather.10.cloned.1.call-update) | async-done | bytes 4194320 | tf_op jit(solution)/shard_map/all_gather | solution.py:20
  119.0 7.4 %convert_multiply_fusion.2 = f32[768,1024]{1,0:T(8,128)} fusion(bf16[768,1024]{1,0:T(8,128)(2,1)} %convolution_convert_fusion.2, bf16[2048,1024]{1,0:T(8,128)(2,1)} %all-gather.10.cloned.1.call-done, bf16[1,768,2048]{2,1,0:T(8,128)(2,1)S(1)} %copy-done, f32[2048]{0:T(1024)S(1)} %copy-done.1, f32[768]{0:T(1024)S(1)} %add_rsqrt_fusion), kind=kOutput, calls=%fused_computation.6 | convolution fusion | flops 3230662656 | bytes 12069888 | tf_op jit(solution)/shard_map/dot_general | solution.py:16
  126.3 47.1 %all-gather.6.cloned.1.call-done = bf16[2048,1024]{1,0:T(8,128)(2,1)} async-done(((bf16[512,1024]{1,0:T(8,128)(2,1)}), bf16[2048,1024]{1,0:T(8,128)(2,1)}) %all-gather.6.cloned.1.call-update) | async-done | bytes 4194320 | tf_op jit(solution)/shard_map/all_gather | solution.py:18
  173.4 9.4 %multiply_convert_fusion = bf16[768,1024]{1,0:T(8,128)(2,1)} fusion(f32[768,1024]{1,0:T(8,128)} %convert_multiply_fusion.2, f32[1024]{0:T(1024)S(1)} %bitcast.19, f32[1024]{0:T(1024)S(1)} %bitcast.18, f32[1024]{0:T(1024)S(1)} %bitcast.17, bf16[2048,1024]{1,0:T(8,128)(2,1)} %all-gather.6.cloned.1.call-done, bf16[1,768,2048]{2,1,0:T(8,128)(2,1)S(1)} %copy-done, ...), kind=kOutput, calls=%fused_computation.5 | convolution fusion | flops 3234594816 | bytes 12082176 | tf_op jit(solution)/shard_map/dot_general | solution.py:16
  182.8 0.0 all-gather.12.cloned.1.call-update
  182.8 44.9 %all-gather.14.cloned.1.call-done = bf16[2048,1024]{1,0:T(8,128)(2,1)} async-done(((bf16[512,1024]{1,0:T(8,128)(2,1)}), bf16[2048,1024]{1,0:T(8,128)(2,1)}) %all-gather.14.cloned.1.call-update) | async-done | bytes 4194320 | tf_op jit(solution)/shard_map/all_gather | solution.py:36
  227.7 13.5 %all-gather.12.cloned.1.call-done = bf16[768,2048]{1,0:T(8,128)(2,1)} async-done(((bf16[768,1024]{1,0:T(8,128)(2,1)}), bf16[768,2048]{1,0:T(8,128)(2,1)}) %all-gather.12.cloned.1.call-update) | async-done | bytes 3145744 | tf_op jit(solution)/shard_map/all_gather | solution.py:33
  241.2 7.7 %fusion.3 = bf16[1,768,1024]{2,1,0:T(8,128)(2,1)} fusion(bf16[768,2048]{1,0:T(8,128)(2,1)} %all-gather.12.cloned.1.call-done, bf16[2048,1024]{1,0:T(8,128)(2,1)} %all-gather.14.cloned.1.call-done), kind=kOutput, calls=%fused_computation.11 | convolution fusion | flops 3222011904 | bytes 8912896 | tf_op jit(solution)/shard_map/dot_general | solution.py:34
  (1 shorter events, 0.0 us)
Async XLA Ops:
  6.5 3.8 %copy-start = (bf16[1,768,2048]{2,1,0:T(8,128)(2,1)S(1)}, bf16[1,768,2048]{2,1,0:T(8,128)(2,1)}, u32[]{:S(2)}) copy-start(bf16[1,768,2048]{2,1,0:T(8,128)(2,1)} %param.7) | copy-start | bytes 9437188
  6.5 58.0 %all-gather.8.cloned.1.call-start = ((), (), s32[]{:S(2)}) async-start(), calls=%async_computation.1 | async-start | bytes 5242880 | tf_op jit(solution)/shard_map/all_gather | solution.py:19
  7.3 57.3 %copy-start.1 = (f32[2048]{0:T(1024)S(1)}, f32[2048]{0:T(1024)}, u32[]{:S(2)}) copy-start(f32[2048]{0:T(1024)} %param.8) | copy-start | bytes 24580
  7.3 111.7 %all-gather.10.cloned.1.call-start = ((), (), s32[]{:S(2)}) async-start(), calls=%async_computation.2 | async-start | bytes 5242880 | tf_op jit(solution)/shard_map/all_gather | solution.py:20
  8.0 165.4 %all-gather.6.cloned.1.call-start = ((), (), s32[]{:S(2)}) async-start(), calls=%async_computation | async-start | bytes 5242880 | tf_op jit(solution)/shard_map/all_gather | solution.py:18
  8.8 219.0 %all-gather.14.cloned.1.call-start = ((), (), s32[]{:S(2)}) async-start(), calls=%async_computation.4 | async-start | bytes 5242880 | tf_op jit(solution)/shard_map/all_gather | solution.py:36
  9.3 231.9 %all-gather.12.cloned.1.call-start = ((), (), s32[]{:S(2)}) async-start(), calls=%async_computation.3 | async-start | bytes 4718592 | tf_op jit(solution)/shard_map/all_gather | solution.py:33
Sparse Core Ops, SparseCore 0:
  9.2 55.2 all-gather.7
  66.3 52.5 all-gather.9
  120.8 52.5 all-gather.5
  175.1 52.5 all-gather.13
  229.1 12.1 all-gather.11
where the time goes:
time: 256 us; the launch traced here: 255 us
  waiting for transfers between devices  209 us (82%)
  matrix products  31.3 us (12%)
  between operations  13.2 us (5%)
    all_gather x1, waiting for transfers between devices, local(): inner = add_piece(lax.all_gather(inner_weight, 'fs', axis=0, tiled=True))  53.5 us
    all_gather x1, waiting for transfers between devices, local(): value = add_piece(lax.all_gather(value_weight, 'fs', axis=0, tiled=True))  47.6 us
    all_gather x1, waiting for transfers between devices, local(): outer = add_piece(lax.all_gather(outer_weight, 'fs', axis=0, tiled=True))  47.1 us
    all_gather x1, waiting for transfers between devices, local(): lax.all_gather(out_weight, 'fs', axis=0, tiled=True)  44.9 us
    dot_general x3, matrix products, add_piece(): return jnp.dot(normed, piece, preferred_element_type=jnp.float32)  23.6 us
    all_gather x1, waiting for transfers between devices, local(): everything = lax.all_gather(gated, 'tp', axis=1, tiled=True)  13.5 us
    dot_general x1, matrix products, local(): jnp.dot(everything, lax.all_gather(out_weight, 'fs', axis=0, tiled=True),...  7.7 us
  transfers between devices with their start and end apart: 5, of which 5 were waited for; matrix products, arithmetic and copies ran while one was open for 10% of the time, Pallas kernels for 0%

commit v1 on v0

--- a/solution.py
+++ b/solution.py
@@ -17,7 +17,11 @@
 
     outer = add_piece(lax.all_gather(outer_weight, "fs", axis=0, tiled=True))
     inner = add_piece(lax.all_gather(inner_weight, "fs", axis=0, tiled=True))
-    value = add_piece(lax.all_gather(value_weight, "fs", axis=0, tiled=True))
+    value = add_piece(
+        jnp.concatenate(
+            lax.all_to_all(jnp.stack([value_weight] * lax.axis_size("fs")), "fs", 0, 0), axis=0
+        )
+    )
     outer = outer.astype(jnp.bfloat16)
     inner = inner.astype(jnp.bfloat16)
     value = value.astype(jnp.bfloat16)

time: 256 us -> 237 us (0.926)
  waiting for transfers between devices: 209 us -> 182 us
  starting transfers between devices: 0.15 us -> 5.53 us
    all_gather x1 -> x0, waiting for transfers between devices: 47.6 us -> none  [local(): value = add_piece(lax.all_gather(value_weight, 'fs', axis=0, tiled=True))]
    all_gather x1, waiting for transfers between devices: 53.5 us -> 80.9 us  [local(): inner = add_piece(lax.all_gather(inner_weight, 'fs', axis=0, tiled=True))]
    all_gather x1, waiting for transfers between devices: 47.1 us -> 40.6 us  [local(): outer = add_piece(lax.all_gather(outer_weight, 'fs', axis=0, tiled=True))]
    all_to_all x0 -> x1, starting transfers between devices: none -> 5.45 us  [local(): lax.all_to_all(jnp.stack([value_weight] * lax.axis_size('fs')), 'fs', 0, 0)]
  transfers between devices with their start and end apart: 5 -> 5, of which waited for: 5 -> 4; matrix products, arithmetic and copies ran while one was open for 10% -> 12% of each run, Pallas kernels for 0% -> 0%
where the time goes in v1:
time: 237 us; the launch traced here: 236 us
  waiting for transfers between devices  182 us (77%)
  matrix products  31.5 us (13%)
  between operations  13.1 us (6%)
  starting transfers between devices  5.53 us (2%)
  local copies, waits for them, and re-layouts  3.41 us (1%)
    all_gather x1, waiting for transfers between devices, local(): inner = add_piece(lax.all_gather(inner_weight, 'fs', axis=0, tiled=True))  80.9 us
    all_gather x1, waiting for transfers between devices, local(): lax.all_gather(out_weight, 'fs', axis=0, tiled=True)  45.1 us
    all_gather x1, waiting for transfers between devices, local(): outer = add_piece(lax.all_gather(outer_weight, 'fs', axis=0, tiled=True))  40.6 us
    dot_general x3, matrix products, add_piece(): return jnp.dot(normed, piece, preferred_element_type=jnp.float32)  23.8 us
    all_gather x1, waiting for transfers between devices, local(): everything = lax.all_gather(gated, 'tp', axis=1, tiled=True)  13.5 us
    dot_general x1, matrix products, local(): jnp.dot(everything, lax.all_gather(out_weight, 'fs', axis=0, tiled=True),...  7.7 us
    all_to_all x1, starting transfers between devices, local(): lax.all_to_all(jnp.stack([value_weight] * lax.axis_size('fs')), 'fs', 0, 0)  5.45 us
  transfers between devices with their start and end apart: 5, of which 4 were waited for; matrix products, arithmetic and copies ran while one was open for 12% of the time, Pallas kernels for 0%

profile of v1, /device:TPU:0, one launch (start us, length us, event | category | flops | bytes accessed | tf_op | source)
XLA Modules:
  0.0 236.4 jit_solution(16711429653905321569)
XLA Ops:
  6.5 0.0 copy-start.1
  6.5 0.0 all-gather.7.cloned.1.call-start
  6.5 0.7 all-gather.7.cloned.1.call-update
  7.3 0.0 all-gather.5.cloned.1.call-start
  7.3 0.7 all-gather.5.cloned.1.call-update
  8.0 0.0 all-gather.11.cloned.1.call-start
  8.1 0.7 all-gather.11.cloned.1.call-update
  8.7 0.0 copy-done.1
  8.8 2.5 %stack.2 = bf16[4,512,1024]{2,1,0:T(8,128)(2,1)} broadcast(bf16[512,1024]{1,0:T(8,128)(2,1)S(1)} %copy-done.1), dimensions={1,2} | broadcast | bytes 5242880 | tf_op jit(solution)/shard_map/stack | solution.py:22
  11.2 0.0 copy-start
  11.2 5.5 %all-to-all-start = ((bf16[4,512,1024]{2,1,0:T(8,128)(2,1)}), bf16[4,512,1024]{2,1,0:T(8,128)(2,1)}, u32[]{:S(2)}, u32[]{:S(2)}) async-start(bf16[4,512,1024]{2,1,0:T(8,128)(2,1)} %stack.2), calls=%async_computation | async-start | bytes 8388608 | tf_op jit(solution)/shard_map/all_to_all | solution.py:22
  16.7 0.0 copy-start.2
  16.7 0.0 all-gather.9.cloned.1.call-start
  16.7 0.9 constant_dynamic-slice_fusion
  17.6 0.0 copy-done
  17.6 0.7 fusion.2
  18.3 80.9 %all-gather.7.cloned.1.call-done = bf16[2048,1024]{1,0:T(8,128)(2,1)} async-done(((bf16[512,1024]{1,0:T(8,128)(2,1)}), bf16[2048,1024]{1,0:T(8,128)(2,1)}) %all-gather.7.cloned.1.call-update) | async-done | bytes 4194320 | tf_op jit(solution)/shard_map/all_gather | solution.py:19
  99.2 0.0 copy-done.2
  99.2 6.8 %convolution_convert_fusion.1 = bf16[768,1024]{1,0:T(8,128)(2,1)} fusion(bf16[2048,1024]{1,0:T(8,128)(2,1)} %all-gather.7.cloned.1.call-done, bf16[1,768,2048]{2,1,0:T(8,128)(2,1)S(1)} %copy-done, f32[2048]{0:T(1024)S(1)} %copy-done.2, f32[768]{0:T(1024)S(1)} %add_rsqrt_fusion), kind=kOutput, calls=%fused_computation.17 | convolution fusion | flops 3228303360 | bytes 8924160 | tf_op jit(solution)/shard_map/dot_general | solution.py:16
  106.0 0.0 all-to-all-done
  106.0 7.6 %convert_multiply_fusion.1 = f32[768,1024]{1,0:T(8,128)} fusion(bf16[768,1024]{1,0:T(8,128)(2,1)} %convolution_convert_fusion.1, bf16[2048,1024]{1,0:T(8,128)(2,1)} %bitcast.3, bf16[1,768,2048]{2,1,0:T(8,128)(2,1)S(1)} %copy-done, f32[2048]{0:T(1024)S(1)} %copy-done.2, f32[768]{0:T(1024)S(1)} %add_rsqrt_fusion), kind=kOutput, calls=%fused_computation.12 | convolution fusion | flops 3230662656 | bytes 12069888 | tf_op jit(solution)/shard_map/dot_general | solution.py:16
  113.6 40.6 %all-gather.5.cloned.1.call-done = bf16[2048,1024]{1,0:T(8,128)(2,1)} async-done(((bf16[512,1024]{1,0:T(8,128)(2,1)}), bf16[2048,1024]{1,0:T(8,128)(2,1)}) %all-gather.5.cloned.1.call-update) | async-done | bytes 4194320 | tf_op jit(solution)/shard_map/all_gather | solution.py:18
  154.2 9.4 %multiply_convert_fusion = bf16[768,1024]{1,0:T(8,128)(2,1)} fusion(f32[768,1024]{1,0:T(8,128)} %convert_multiply_fusion.1, f32[1024]{0:T(1024)S(1)} %bitcast.34, f32[1024]{0:T(1024)S(1)} %bitcast.33, f32[1024]{0:T(1024)S(1)} %bitcast.32, bf16[2048,1024]{1,0:T(8,128)(2,1)} %all-gather.5.cloned.1.call-done, bf16[1,768,2048]{2,1,0:T(8,128)(2,1)S(1)} %copy-done, ...), kind=kOutput, calls=%fused_computation.11 | convolution fusion | flops 3234594816 | bytes 12082176 | tf_op jit(solution)/shard_map/dot_general | solution.py:16
  163.6 0.0 all-gather.9.cloned.1.call-update
  163.6 45.1 %all-gather.11.cloned.1.call-done = bf16[2048,1024]{1,0:T(8,128)(2,1)} async-done(((bf16[512,1024]{1,0:T(8,128)(2,1)}), bf16[2048,1024]{1,0:T(8,128)(2,1)}) %all-gather.11.cloned.1.call-update) | async-done | bytes 4194320 | tf_op jit(solution)/shard_map/all_gather | solution.py:40
  208.6 13.5 %all-gather.9.cloned.1.call-done = bf16[768,2048]{1,0:T(8,128)(2,1)} async-done(((bf16[768,1024]{1,0:T(8,128)(2,1)}), bf16[768,2048]{1,0:T(8,128)(2,1)}) %all-gather.9.cloned.1.call-update) | async-done | bytes 3145744 | tf_op jit(solution)/shard_map/all_gather | solution.py:37
  222.2 7.7 %fusion.17 = bf16[1,768,1024]{2,1,0:T(8,128)(2,1)} fusion(bf16[768,2048]{1,0:T(8,128)(2,1)} %all-gather.9.cloned.1.call-done, bf16[2048,1024]{1,0:T(8,128)(2,1)} %all-gather.11.cloned.1.call-done), kind=kOutput, calls=%fused_computation.19 | convolution fusion | flops 3222011904 | bytes 8912896 | tf_op jit(solution)/shard_map/dot_general | solution.py:38
  (1 shorter events, 0.0 us)
Async XLA Ops:
  6.5 2.2 copy-start.1
  6.5 92.7 %all-gather.7.cloned.1.call-start = ((), (), s32[]{:S(2)}) async-start(), calls=%async_computation.2 | async-start | bytes 5242880 | tf_op jit(solution)/shard_map/all_gather | solution.py:19
  7.3 146.9 %all-gather.5.cloned.1.call-start = ((), (), s32[]{:S(2)}) async-start(), calls=%async_computation.1 | async-start | bytes 5242880 | tf_op jit(solution)/shard_map/all_gather | solution.py:18
  8.0 200.6 %all-gather.11.cloned.1.call-start = ((), (), s32[]{:S(2)}) async-start(), calls=%async_computation.4 | async-start | bytes 5242880 | tf_op jit(solution)/shard_map/all_gather | solution.py:40
  11.2 6.4 %copy-start = (bf16[1,768,2048]{2,1,0:T(8,128)(2,1)S(1)}, bf16[1,768,2048]{2,1,0:T(8,128)(2,1)}, u32[]{:S(2)}) copy-start(bf16[1,768,2048]{2,1,0:T(8,128)(2,1)} %param.7) | copy-start | bytes 9437188
  11.2 94.8 %all-to-all-start = ((bf16[4,512,1024]{2,1,0:T(8,128)(2,1)}), bf16[4,512,1024]{2,1,0:T(8,128)(2,1)}, u32[]{:S(2)}, u32[]{:S(2)}) async-start(bf16[4,512,1024]{2,1,0:T(8,128)(2,1)} %stack.2), calls=%async_computation | async-start | bytes 8388608 | tf_op jit(solution)/shard_map/all_to_all | solution.py:22
  16.7 82.5 %copy-start.2 = (f32[2048]{0:T(1024)S(1)}, f32[2048]{0:T(1024)}, u32[]{:S(2)}) copy-start(f32[2048]{0:T(1024)} %param.8) | copy-start | bytes 24580
  16.7 205.5 %all-gather.9.cloned.1.call-start = ((), (), s32[]{:S(2)}) async-start(), calls=%async_computation.3 | async-start | bytes 4718592 | tf_op jit(solution)/shard_map/all_gather | solution.py:37
Sparse Core Ops, SparseCore 0:
  9.2 89.9 all-gather.6
  101.0 53.1 all-gather.4
  156.0 52.5 all-gather.10
  210.0 12.1 all-gather.8
